TPU v7x, 32 devices: a whole 2x2x4 slice. The times are simulated.
32 devices in a mesh: ra: 8 (over z, y), cb: 4 (over x, core).
Axes of the slice: x: 2, y: 2, z: 4, core: 2. Of those that a mesh axis runs over, the one named last changes fastest.
Arguments:
- tokens: bfloat16 [256, 3072], P(None, 'ra'), may hold values from -8 to 8, as said below
- first_gain: float32 [3072], P('ra'), may hold values from 0.1 to 1.9
- first_gate: float32 [3072, 8192], P('ra', 'cb'), may hold values from -0.109375 to 0.109375
- first_up: float32 [3072, 8192], P('ra', 'cb'), may hold values from -0.109375 to 0.109375
- first_down: float32 [8192, 3072], P('cb', 'ra'), may hold values from -0.0625 to 0.0625
- first_gate_scale: float32 [8192], P('cb'), may hold values from 0.5 to 2
- first_up_scale: float32 [8192], P('cb'), may hold values from 0.5 to 2
- first_down_scale: float32 [3072], P('ra'), may hold values from 0.5 to 2
- second_gain: float32 [3072], P('ra'), may hold values from 0.1 to 1.9
- second_gate: float32 [3072, 8192], P('ra', 'cb'), may hold values from -0.109375 to 0.109375
- second_up: float32 [3072, 8192], P('ra', 'cb'), may hold values from -0.109375 to 0.109375
- second_down: float32 [8192, 3072], P('cb', 'ra'), may hold values from -0.0625 to 0.0625
- second_gate_scale: float32 [8192], P('cb'), may hold values from 0.5 to 2
- second_up_scale: float32 [8192], P('cb'), may hold values from 0.5 to 2
- second_down_scale: float32 [3072], P('ra'), may hold values from 0.5 to 2
Outputs:
- mixed: bfloat16 [256, 3072], P(None, 'ra')
Inputs may be any that keep to these rules, and one draw needn't show every extreme that they name: The features come in groups of 64 with different magnitudes, and tokens differ in magnitude.
All inputs are finite; a program needn't handle non-finite values.
Results may differ from a plain program's by a relative error of at most 0.0093.
Values may be sent and summed in bfloat16 or wider, within the bound.
A program may use at most 64 MiB of HBM per device.

v0:
```python
import jax
import jax.numpy as jnp
from jax import lax
from jax.sharding import PartitionSpec as P

D = 3072


def half_step(stream_in, gain, w_gate, w_up, w_down, gate_scale, up_scale, down_scale):
    stream = stream_in.astype(jnp.float32)
    squares = jnp.sum(stream * stream, axis=1)
    shaped = (stream * gain[None, :]).astype(jnp.bfloat16)
    gate_part = jnp.dot(shaped, w_gate.astype(jnp.bfloat16), preferred_element_type=jnp.float32)
    up_part = jnp.dot(shaped, w_up.astype(jnp.bfloat16), preferred_element_type=jnp.float32)
    squares, gate_sum, up_sum = lax.psum((squares, gate_part, up_part), "ra")
    inverse = lax.rsqrt(squares / D + 1e-06)[:, None]
    gate_full = inverse * gate_scale[None, :] * gate_sum
    up_full = inverse * up_scale[None, :] * up_sum
    hidden = (jax.nn.silu(gate_full) * up_full).astype(jnp.bfloat16)
    down_part = jnp.dot(hidden, w_down.astype(jnp.bfloat16), preferred_element_type=jnp.float32)
    down_sum = lax.psum(down_part, "cb")
    return (stream + 0.5 * down_scale[None, :] * down_sum).astype(jnp.bfloat16)


def body(
    tokens,
    first_gain,
    first_gate,
    first_up,
    first_down,
    first_gate_scale,
    first_up_scale,
    first_down_scale,
    second_gain,
    second_gate,
    second_up,
    second_down,
    second_gate_scale,
    second_up_scale,
    second_down_scale,
):
    middle = half_step(
        tokens,
        first_gain,
        first_gate,
        first_up,
        first_down,
        first_gate_scale,
        first_up_scale,
        first_down_scale,
    )
    return half_step(
        middle,
        second_gain,
        second_gate,
        second_up,
        second_down,
        second_gate_scale,
        second_up_scale,
        second_down_scale,
    )


def solution(mesh):
    return jax.shard_map(
        body,
        mesh=mesh,
        in_specs=(
            P(None, "ra"),
            P("ra"),
            P("ra", "cb"),
            P("ra", "cb"),
            P("cb", "ra"),
            P("cb"),
            P("cb"),
            P("ra"),
            P("ra"),
            P("ra", "cb"),
            P("ra", "cb"),
            P("cb", "ra"),
            P("cb"),
            P("cb"),
            P("ra"),
        ),
        out_specs=P(None, "ra"),
        check_vma=False,
    )
```

profile of v0, /device:TPU:0, one launch (start us, length us, event | category | flops | bytes accessed | tf_op | source)
XLA Modules:
  0.0 416.3 jit_solution(14474829780918791749)
XLA Ops:
  6.5 4.2 %fusion.10 = f32[256,2048]{1,0:T(8,128)} fusion(f32[384,2048]{1,0:T(8,128)} %param.17, bf16[256,384]{1,0:T(8,128)(2,1)} %param.15, f32[384]{0:T(512)} %param.16), kind=kOutput, calls=%fused_computation.12 | convolution fusion | flops 403734528 | bytes 5441024 | tf_op jit(solution)/shard_map/dot_general | solution.py:13
  10.8 2.0 fusion.8
  12.8 0.0 all-reduce.13.cloned.1.call-update
  12.8 0.0 all-reduce.7.cloned.1.call-start
  12.9 0.1 fusion.12
  13.0 24.3 %psum.56 = f32[256]{0:T(256)S(1)} all-reduce(f32[256]{0:T(256)S(1)} %fusion.12), channel_id=1, replica_groups=mesh['ra'=8,'cb'=4] {'ra'}, use_global_device_ids=true, to_apply=%region_1.0 | all-reduce | flops 256 | bytes 2048 | tf_op jit(solution)/shard_map/psum | solution.py:15
  37.3 135.1 %all-reduce.13.cloned.1.call-done = (f32[256,2048]{1,0:T(8,128)}, f32[256,2048]{1,0:T(8,128)}) async-done(((f32[256,2048]{1,0:T(8,128)}, f32[256,2048]{1,0:T(8,128)}), (f32[256,2048]{1,0:T(8,128)}, f32[256,2048]{1,0:T(8,128)})) %all-reduce.13.cloned.1.call-update) | async-done | bytes 4194320 | tf_op jit(solution)/shard_map/psum | solution.py:15
  172.4 5.1 %fusion.6 = f32[256,384]{1,0:T(8,128)} fusion(f32[2048,384]{1,0:T(8,128)} %param.19, f32[256,2048]{1,0:T(8,128)} %get-tuple-element.7, f32[256,2048]{1,0:T(8,128)} %get-tuple-element.8, f32[2048]{0:T(1024)S(1)} %copy-done.9, f32[2048]{0:T(1024)S(1)} %copy-done.10, f32[256]{0:T(256)S(1)} %add_rsqrt_fusion.1), kind=kOutput, calls=%fused_computation.8 | convolution fusion | flops 408682496 | bytes 7750656 | tf_op jit(solution)/shard_map/dot_general | solution.py:20
  177.5 0.0 all-reduce.7.cloned.1.call-update
  177.6 0.0 all-reduce.11.cloned.1.call-start
  177.6 31.9 %all-reduce.7.cloned.1.call-done = f32[256,384]{1,0:T(8,128)} async-done(((f32[256,384]{1,0:T(8,128)}), f32[256,384]{1,0:T(8,128)}) %all-reduce.7.cloned.1.call-update) | async-done | bytes 393232 | tf_op jit(solution)/shard_map/psum | solution.py:21
  209.5 1.1 fusion.15
  210.7 0.0 copy-start.3
  210.7 2.0 fusion.2
  212.7 0.3 copy-done.3
  213.1 2.1 fusion.4
  215.2 0.0 all-reduce.11.cloned.1.call-update
  215.2 0.0 all-reduce.9.cloned.1.call-start
  215.2 22.8 %psum.60 = f32[256]{0:T(256)S(1)} all-reduce(f32[256]{0:T(256)S(1)} %get-tuple-element.9), channel_id=1, replica_groups=mesh['ra'=8,'cb'=4] {'ra'}, use_global_device_ids=true, to_apply=%region_6.7 | all-reduce | flops 256 | bytes 2048 | tf_op jit(solution)/shard_map/psum | solution.py:15
  238.0 133.9 %all-reduce.11.cloned.1.call-done = (f32[256,2048]{1,0:T(8,128)}, f32[256,2048]{1,0:T(8,128)}) async-done(((f32[256,2048]{1,0:T(8,128)}, f32[256,2048]{1,0:T(8,128)}), (f32[256,2048]{1,0:T(8,128)}, f32[256,2048]{1,0:T(8,128)})) %all-reduce.11.cloned.1.call-update) | async-done | bytes 4194320 | tf_op jit(solution)/shard_map/psum | solution.py:15
  372.0 4.1 fusion
  376.0 0.0 all-reduce.9.cloned.1.call-update
  376.1 31.9 %all-reduce.9.cloned.1.call-done = f32[256,384]{1,0:T(8,128)} async-done(((f32[256,384]{1,0:T(8,128)}), f32[256,384]{1,0:T(8,128)}) %all-reduce.9.cloned.1.call-update) | async-done | bytes 393232 | tf_op jit(solution)/shard_map/psum | solution.py:21
  408.0 1.7 fusion.17
  (29 shorter events, 0.1 us)
Async XLA Ops:
  6.5 4.2 %copy-start = (bf16[256,384]{1,0:T(8,128)(2,1)S(1)}, bf16[256,384]{1,0:T(8,128)(2,1)}, u32[]{:S(2)}) copy-start(bf16[256,384]{1,0:T(8,128)(2,1)} %param.15) | copy-start | bytes 589828
  6.5 4.2 %copy-start.4 = (f32[384]{0:T(512)S(1)}, f32[384]{0:T(512)}, u32[]{:S(2)}) copy-start(f32[384]{0:T(512)} %param.16) | copy-start | bytes 4612
  6.5 4.2 %copy-start.1 = (f32[384,2048]{1,0:T(8,128)S(1)}, f32[384,2048]{1,0:T(8,128)}, u32[]{:S(2)}) copy-start(f32[384,2048]{1,0:T(8,128)} %param.18) | copy-start | bytes 9437188
  6.5 165.9 %all-reduce.13.cloned.1.call-start = ((), (), s32[]{:S(2)}) async-start(), calls=%async_computation.3 | async-start | bytes 8388608 | tf_op jit(solution)/shard_map/psum | solution.py:15
  12.8 159.6 %copy-start.9 = (f32[2048]{0:T(1024)S(1)}, f32[2048]{0:T(1024)}, u32[]{:S(2)}) copy-start(f32[2048]{0:T(1024)} %param.21) | copy-start | bytes 24580
  12.8 159.6 %copy-start.10 = (f32[2048]{0:T(1024)S(1)}, f32[2048]{0:T(1024)}, u32[]{:S(2)}) copy-start(f32[2048]{0:T(1024)} %param.20) | copy-start | bytes 24580
  12.8 196.7 %all-reduce.7.cloned.1.call-start = ((), (), s32[]{:S(2)}) async-start(), calls=%async_computation | async-start | bytes 786432 | tf_op jit(solution)/shard_map/psum | solution.py:21
  172.4 5.2 %copy-start.6 = (f32[384]{0:T(512)S(1)}, f32[384]{0:T(512)}, u32[]{:S(2)}) copy-start(f32[384]{0:T(512)} %param.22) | copy-start | bytes 4612
  172.4 38.3 %copy-start.2 = (f32[384,2048]{1,0:T(8,128)S(1)}, f32[384,2048]{1,0:T(8,128)}, u32[]{:S(2)}) copy-start(f32[384,2048]{1,0:T(8,128)} %param.25) | copy-start | bytes 9437188
  172.4 38.3 %copy-start.5 = (f32[384]{0:T(512)S(1)}, f32[384]{0:T(512)}, u32[]{:S(2)}) copy-start(f32[384]{0:T(512)} %param.23) | copy-start | bytes 4612
  177.6 194.4 %all-reduce.11.cloned.1.call-start = ((), (), s32[]{:S(2)}) async-start(), calls=%async_computation.2 | async-start | bytes 8388608 | tf_op jit(solution)/shard_map/psum | solution.py:15
  210.7 2.4 copy-start.3
  215.2 156.8 %copy-start.8 = (f32[2048,384]{1,0:T(8,128)S(1)}, f32[2048,384]{1,0:T(8,128)}, u32[]{:S(2)}) copy-start(f32[2048,384]{1,0:T(8,128)} %param.26) | copy-start | bytes 9437188
  215.2 156.8 %copy-start.11 = (f32[2048]{0:T(1024)S(1)}, f32[2048]{0:T(1024)}, u32[]{:S(2)}) copy-start(f32[2048]{0:T(1024)} %param.28) | copy-start | bytes 24580
  215.2 156.8 %copy-start.12 = (f32[2048]{0:T(1024)S(1)}, f32[2048]{0:T(1024)}, u32[]{:S(2)}) copy-start(f32[2048]{0:T(1024)} %param.27) | copy-start | bytes 24580
  215.2 192.8 %all-reduce.9.cloned.1.call-start = ((), (), s32[]{:S(2)}) async-start(), calls=%async_computation.1 | async-start | bytes 786432 | tf_op jit(solution)/shard_map/psum | solution.py:21
  372.0 4.1 copy-start.7
Sparse Core Ops, SparseCore 0:
  13.0 159.4 all-reduce.12
  177.7 31.7 all-reduce.6
  215.3 156.5 all-reduce.10
  376.2 31.7 all-reduce.8
where the time goes:
time: 417 us; the launch traced here: 416 us
  waiting for transfers between devices  333 us (80%)
  blocking collectives  47 us (11%)
  matrix products  19.6 us (5%)
  between operations  13.2 us (3%)
    psum x2, waiting for transfers between devices, half_step(): squares, gate_sum, up_sum = lax.psum((squares, gate_part, up_part), 'ra')  269 us
    psum x2, waiting for transfers between devices, half_step(): down_sum = lax.psum(down_part, 'cb')  63.8 us
    psum x2, blocking collectives, half_step(): squares, gate_sum, up_sum = lax.psum((squares, gate_part, up_part), 'ra')  47 us
    dot_general x2, matrix products, half_step(): jnp.dot(hidden, w_down.astype(jnp.bfloat16), preferred_element_type=jnp.f...  9.19 us
  transfers between devices with their start and end apart: 4, of which 4 were waited for; matrix products, arithmetic and copies ran while one was open for 0% of the time, Pallas kernels for 0%

commit v1 on v0

v1 whole, which is shorter than its diff:
```python
import functools
import jax
import jax.numpy as jnp
from jax import lax
from jax.experimental import pallas as pl
from jax.experimental.pallas import tpu as pltpu
from jax.sharding import PartitionSpec as P

MESH = pl.DeviceIdType.MESH
LANES = 128
CHUNK = 32
LAGS = (0, 1, 2, 3, 4, 5, 6, 7, 8)


def bits_of(n):
    return n.bit_length() - 1


def kernel(cfg, *refs):
    ra, cb, chunk, chunks, width, hid, model, lags = cfg
    (tok, gain1, gain2, gsc1, usc1, dsc1, gsc2, usc2, dsc2, g1, u1, d1, g2, u2, d2, out) = refs[:16]
    refs = refs[16:]
    nra, ncb = bits_of(ra), bits_of(cb)
    (fg, fu, fd, wgu, wd, stream, gains, gsc, usc, dsc, sqa, hb, load_sem) = refs[:13]
    refs = refs[13:]
    snd, rcv, own = refs[:nra], refs[nra : 2 * nra], refs[2 * nra : 3 * nra]
    refs = refs[3 * nra :]
    csnd, crcv = refs[0], refs[1]
    rs_s, rs_r, ag_s, ag_r, cb_s, cb_r = refs[2:]
    hl = hid // ra // LANES
    nl = 2 * hl

    me_r = lax.axis_index("ra")
    me_c = lax.axis_index("cb")
    rbit = [(me_r // (1 << k)) % 2 for k in range(nra)]
    cbit = [(me_c // (1 << k)) % 2 for k in range(ncb)]
    ra_peer = [me_r + (1 - 2 * rbit[k]) * (1 << k) for k in range(nra)]
    cb_peer = [me_c + (1 - 2 * cbit[k]) * (1 << k) for k in range(ncb)]
    pos = 0
    for k in range(nra):
        pos = pos + rbit[k] * (1 << (nra - 1 - k))

    loads = []
    for layer, (g, u, d) in enumerate(((g1, u1, d1), (g2, u2, d2))):
        for q, (src, dst) in enumerate(((g, fg), (u, fu), (d, fd))):
            copy = pltpu.make_async_copy(src, dst.at[layer], load_sem.at[layer * 3 + q])
            copy.start()
            loads.append(copy)

    barrier = pltpu.get_barrier_semaphore()
    for k in range(nra):
        pl.semaphore_signal(barrier, inc=1, device_id=(ra_peer[k], me_c), device_id_type=MESH)
    for k in range(ncb):
        pl.semaphore_signal(barrier, inc=1, device_id=(me_r, cb_peer[k]), device_id_type=MESH)

    stream[0] = tok[...]
    gains[0] = gain1[...]
    gains[1] = gain2[...]
    dsc[0] = dsc1[...] * 0.5
    dsc[1] = dsc2[...] * 0.5
    for src, dst, layer in ((gsc1, gsc, 0), (gsc2, gsc, 1), (usc1, usc, 0), (usc2, usc, 1)):
        for i in range(hid // LANES):
            dst[layer, i] = src[i : i + 1, :]

    def rev(j):
        r = 0
        for k in range(nra):
            r |= ((j >> k) & 1) << (nra - 1 - k)
        return r

    hw = hl * LANES

    def convert_cols(layer, src, half):
        for j in range(ra):
            r = rev(j)
            wgu[layer, j, :, half * hw : (half + 1) * hw] = src[layer, :, r * hw : (r + 1) * hw].astype(jnp.bfloat16)

    def convert_down(layer):
        for j in range(ra):
            r = rev(j)
            wd[layer, j * hw : (j + 1) * hw, :] = fd[layer, r * hw : (r + 1) * hw, :].astype(jnp.bfloat16)

    loads[0].wait()
    convert_cols(0, fg, 0)
    loads[1].wait()
    convert_cols(0, fu, 1)
    pl.semaphore_wait(barrier, nra + ncb)

    def rs_copy(k, c):
        return pltpu.make_async_remote_copy(
            src_ref=snd[k].at[c], dst_ref=rcv[k].at[c], send_sem=rs_s.at[k, c], recv_sem=rs_r.at[k, c],
            device_id=(ra_peer[k], me_c), device_id_type=MESH)

    def ag_copy(a, c):
        span = 1 << a
        part = hb.at[c, pl.ds((pos // span) * (span * hl), span * hl)]
        return pltpu.make_async_remote_copy(
            src_ref=part, dst_ref=part, send_sem=ag_s.at[a, c], recv_sem=ag_r.at[a, c],
            device_id=(ra_peer[nra - 1 - a], me_c), device_id_type=MESH)

    def cb_copy(b, i):
        return pltpu.make_async_remote_copy(
            src_ref=csnd.at[b, i], dst_ref=crcv.at[b, i], send_sem=cb_s.at[b, i], recv_sem=cb_r.at[b, i],
            device_id=(me_r, cb_peer[b]), device_id_type=MESH)

    def put_squares(k, c, sq):
        hi = sq.astype(jnp.bfloat16)
        lo = (sq - hi.astype(jnp.float32)).astype(jnp.bfloat16)
        lane = lax.broadcasted_iota(jnp.int32, sq.shape, 1)
        mixed = jnp.where(lane < LANES // 2, hi.astype(jnp.float32), lo.astype(jnp.float32))
        snd[k][c, (ra >> (k + 1)) * nl] = mixed.astype(jnp.bfloat16)

    def get_squares(k, c):
        v = rcv[k][c, (ra >> (k + 1)) * nl].astype(jnp.float32)
        return sqa[c] + (v + pltpu.roll(v, LANES // 2, 1))

    def first(layer, c):
        s = stream[layer, c].astype(jnp.float32)
        sq = jnp.broadcast_to(jnp.sum(s * s, axis=1, keepdims=True), (chunk, LANES))
        sqa[c] = sq
        put_squares(0, c, sq)
        shaped = (s * gains[layer]).astype(jnp.bfloat16)
        half = ra // 2
        for jj in range(half):
            r = jnp.dot(shaped, wgu[layer, (1 - rbit[0]) * half + jj], preferred_element_type=jnp.float32)
            for q in range(nl):
                snd[0][c, jj * nl + q] = r[:, q * LANES : (q + 1) * LANES].astype(jnp.bfloat16)
        rs_copy(0, c).start()
        for jj in range(half):
            r = jnp.dot(shaped, wgu[layer, rbit[0] * half + jj], preferred_element_type=jnp.float32)
            for q in range(nl):
                own[0][c, jj * nl + q] = r[:, q * LANES : (q + 1) * LANES]

    def reduce(k, layer, c):
        rs_copy(k - 1, c).wait()
        n = (ra >> (k + 1)) * nl
        sq = get_squares(k - 1, c)
        sqa[c] = sq
        put_squares(k, c, sq)
        away = pl.ds((1 - rbit[k]) * n, n)
        snd[k][c, 0:n] = (own[k - 1][c, away] + rcv[k - 1][c, away].astype(jnp.float32)).astype(jnp.bfloat16)
        rs_copy(k, c).start()
        keep = pl.ds(rbit[k] * n, n)
        own[k][c] = own[k - 1][c, keep] + rcv[k - 1][c, keep].astype(jnp.float32)

    def gate(layer, c):
        k = nra - 1
        rs_copy(k, c).wait()
        total = own[k][c] + rcv[k][c, 0:nl].astype(jnp.float32)
        inverse = lax.rsqrt(get_squares(k, c) / model + 1e-06)[None]
        mine = pl.ds(me_r * hl, hl)
        g = inverse * gsc[layer, mine] * total[:hl]
        u = inverse * usc[layer, mine] * total[hl:]
        hidden = (g / (1.0 + jnp.exp(-g))) * u
        hb[c, pl.ds(pos * hl, hl)] = hidden.astype(jnp.bfloat16)
        ag_copy(0, c).start()

    def gather(a, layer, c):
        ag_copy(a - 1, c).wait()
        ag_copy(a, c).start()

    def down(layer, c):
        ag_copy(nra - 1, c).wait()
        h = jnp.concatenate([hb[c, i] for i in range(hid // LANES)], axis=1)
        i = layer * chunks + c
        csnd[0, i] = jnp.dot(h, wd[layer], preferred_element_type=jnp.float32).astype(jnp.bfloat16)
        cb_copy(0, i).start()

    def csum(b, i):
        cb_copy(b, i).wait()
        return csnd[b, i].astype(jnp.float32) + crcv[b, i].astype(jnp.float32)

    def across(b, layer, c):
        i = layer * chunks + c
        csnd[b, i] = csum(b - 1, i).astype(jnp.bfloat16)
        cb_copy(b, i).start()

    def last(layer, c):
        i = layer * chunks + c
        total = csum(ncb - 1, i)
        s = stream[layer, c].astype(jnp.float32)
        stream[layer + 1, c] = (s + dsc[layer] * total).astype(jnp.bfloat16)

    stages = [first]
    stages += [functools.partial(reduce, k) for k in range(1, nra)]
    stages += [gate]
    stages += [functools.partial(gather, a) for a in range(1, nra)]
    stages += [down]
    stages += [functools.partial(across, b) for b in range(1, ncb)]
    stages += [last]
    shift = max(chunks, lags[-1] + 1)

    later = {
        0: lambda: (loads[2].wait(), convert_down(0)),
        1: lambda: (loads[3].wait(), convert_cols(1, fg, 0)),
        2: lambda: (loads[4].wait(), convert_cols(1, fu, 1)),
        3: lambda: (loads[5].wait(), convert_down(1)),
    }

    def tick(t, carry):
        order = [0] + list(range(len(stages) - 1, 0, -1))
        for s in order:
            rel = t - lags[s]
            layer = jnp.where(rel >= shift, 1, 0)
            c = rel - layer * shift

            @pl.when((rel >= 0) & (c < chunks))
            def _(s=s, layer=layer, c=c):
                stages[s](layer, c)

        for at, act in later.items():
            @pl.when(t == at)
            def _(act=act):
                act()

        return carry

    lax.fori_loop(0, shift + chunks + lags[-1], tick, 0)
    out[...] = stream[2]


def fused(cfg, *args):
    ra, cb, chunk, chunks, width, hid, model, lags = cfg
    nra, ncb = bits_of(ra), bits_of(cb)
    (tok, gain1, g1, u1, d1, gs1, us1, ds1, gain2, g2, u2, d2, gs2, us2, ds2) = args
    rows = hid // LANES
    nl = 2 * (hid // ra // LANES)
    bf, f32 = jnp.bfloat16, jnp.float32
    V = pltpu.VMEM
    D = pltpu.SemaphoreType.DMA
    scratch = [
        V((2, width, hid), f32),
        V((2, width, hid), f32),
        V((2, hid, width), f32),
        V((2, ra, width, nl * LANES), bf),
        V((2, hid, width), bf),
        V((3, chunks, chunk, width), bf),
        V((2, 1, width), f32),
        V((2, rows, 1, LANES), f32),
        V((2, rows, 1, LANES), f32),
        V((2, 1, width), f32),
        V((chunks, chunk, LANES), f32),
        V((chunks, rows, chunk, LANES), bf),
        D((6,)),
    ]
    scratch += [V((chunks, (ra >> (k + 1)) * nl + 1, chunk, LANES), bf) for k in range(nra)]
    scratch += [V((chunks, (ra >> (k + 1)) * nl + 1, chunk, LANES), bf) for k in range(nra)]
    scratch += [V((chunks, (ra >> (k + 1)) * nl, chunk, LANES), f32) for k in range(nra)]
    scratch += [V((ncb, 2 * chunks, chunk, width), bf), V((ncb, 2 * chunks, chunk, width), bf)]
    scratch += [D((nra, chunks)), D((nra, chunks)), D((nra, chunks)), D((nra, chunks))]
    scratch += [D((ncb, 2 * chunks)), D((ncb, 2 * chunks))]
    vm = pl.BlockSpec(memory_space=pltpu.VMEM)
    hbm = pl.BlockSpec(memory_space=pl.ANY)
    result = pl.pallas_call(
        functools.partial(kernel, cfg),
        out_shape=jax.ShapeDtypeStruct((chunks, chunk, width), bf),
        in_specs=[vm] * 9 + [hbm] * 6,
        out_specs=vm,
        scratch_shapes=scratch,
        compiler_params=pltpu.CompilerParams(collective_id=0, has_side_effects=True, vmem_limit_bytes=64 * 1000 * 1000),
    )(
        tok.reshape(chunks, chunk, width),
        gain1.reshape(1, width), gain2.reshape(1, width),
        gs1.reshape(rows, LANES), us1.reshape(rows, LANES), ds1.reshape(1, width),
        gs2.reshape(rows, LANES), us2.reshape(rows, LANES), ds2.reshape(1, width),
        g1, u1, d1, g2, u2, d2,
    )
    return result.reshape(chunks * chunk, width)


def plain_half(model, s_in, gain, w_gate, w_up, w_down, gate_scale, up_scale, down_scale):
    stream = s_in.astype(jnp.float32)
    squares = jnp.sum(stream * stream, axis=1)
    shaped = (stream * gain[None, :]).astype(jnp.bfloat16)
    gate_part = jnp.dot(shaped, w_gate.astype(jnp.bfloat16), preferred_element_type=jnp.float32)
    up_part = jnp.dot(shaped, w_up.astype(jnp.bfloat16), preferred_element_type=jnp.float32)
    squares, gate_sum, up_sum = lax.psum((squares, gate_part, up_part), "ra")
    inverse = lax.rsqrt(squares / model + 1e-06)[:, None]
    gate_full = inverse * gate_scale[None, :] * gate_sum
    up_full = inverse * up_scale[None, :] * up_sum
    hidden = (jax.nn.silu(gate_full) * up_full).astype(jnp.bfloat16)
    down_part = jnp.dot(hidden, w_down.astype(jnp.bfloat16), preferred_element_type=jnp.float32)
    down_sum = lax.psum(down_part, "cb")
    return (stream + 0.5 * down_scale[None, :] * down_sum).astype(jnp.bfloat16)


def solution(mesh):
    ra, cb = mesh.shape["ra"], mesh.shape["cb"]

    def body(*args):
        tokens, width = args[0].shape
        hid = args[2].shape[1]
        power = ra & (ra - 1) == 0 and cb & (cb - 1) == 0 and ra > 1 and cb > 1
        if power and hid % (ra * LANES) == 0 and width % LANES == 0 and tokens % CHUNK == 0:
            stages = 2 * bits_of(ra) + bits_of(cb) + 1
            lags = LAGS if len(LAGS) == stages else tuple(range(stages))
            cfg = (ra, cb, CHUNK, tokens // CHUNK, width, hid, width * ra, lags)
            return fused(cfg, *args)
        middle = plain_half(width * ra, *args[:8])
        return plain_half(width * ra, middle, *args[8:])

    col, grid, turned = P("ra"), P("ra", "cb"), P("cb", "ra")
    sub = (col, grid, grid, turned, P("cb"), P("cb"), col)
    return jax.shard_map(
        body, mesh=mesh, in_specs=(P(None, "ra"),) + sub + sub, out_specs=P(None, "ra"), check_vma=False)
```

time: 417 us -> 117 us (0.28)
  waiting for transfers between devices: 333 us -> 0 us
  Pallas kernels: 0 us -> 110 us
  blocking collectives: 47 us -> 0 us
  matrix products: 19.6 us -> 0 us
  between operations: 13.2 us -> 0.01 us
  local copies, waits for them, and re-layouts: 0.39 us -> 6.61 us
    psum x4 -> x0, waiting for transfers between devices: 333 us -> none  [the longest x2 269 us: half_step(): squares, gate_sum, up_sum = lax.psum((squares, gate_part, up_part), 'ra')]
    pallas_call x0 -> x1, Pallas kernels: none -> 110 us  [fused(): pl.pallas_call(functools.partial(kernel, cfg), out_shape=jax.ShapeDtypeSt...]
    psum x2 -> x0, blocking collectives: 47 us -> none  [half_step(): squares, gate_sum, up_sum = lax.psum((squares, gate_part, up_part), 'ra')]
    dot_general x6 -> x0, matrix products: 19.6 us -> none  [the longest x2 9.19 us: half_step(): jnp.dot(hidden, w_down.astype(jnp.bfloat16), preferred_element_type=jnp.f...]
    reshape x0 -> x4, local copies, waits for them, and re-layouts: none -> 4.99 us  [the longest x1 1.26 us: fused(): gain2.reshape(1, width)]
  transfers between devices with their start and end apart: 4 -> 0, of which waited for: 4 -> 0; matrix products, arithmetic and copies ran while one was open for 0% -> 0% of each run, Pallas kernels for 0% -> 0%
where the time goes in v1:
time: 117 us
  Pallas kernels  110 us (94%)
  local copies, waits for them, and re-layouts  6.61 us (6%)
    pallas_call x1, Pallas kernels, fused(): pl.pallas_call(functools.partial(kernel, cfg), out_shape=jax.ShapeDtypeSt...  110 us

profile of v1, /device:TPU:0, one launch (start us, length us, event | category | flops | bytes accessed | tf_op | source)
XLA Modules:
  0.0 116.9 jit_solution(4327943802182647973)
XLA Ops:
  0.0 1.2 %reshape.31.refs_1_ = f32[1,384]{1,0:T(1,128)} reshape(f32[384]{0:T(512)} %param.16) | data formatting | bytes 3072 | tf_op jit(solution)/shard_map/reshape | solution.py:263
  1.2 1.2 %reshape.35.refs_5_ = f32[1,384]{1,0:T(1,128)} reshape(f32[384]{0:T(512)} %param.22) | data formatting | bytes 3072 | tf_op jit(solution)/shard_map/reshape | solution.py:264
  2.5 1.3 %reshape.32.refs_2_ = f32[1,384]{1,0:T(1,128)} reshape(f32[384]{0:T(512)} %param.23) | data formatting | bytes 3072 | tf_op jit(solution)/shard_map/reshape | solution.py:263
  3.7 1.2 %reshape.38.refs_8_ = f32[1,384]{1,0:T(1,128)} reshape(f32[384]{0:T(512)} %param.29) | data formatting | bytes 3072 | tf_op jit(solution)/shard_map/reshape | solution.py:265
  5.0 110.3 %shard_map.145 = bf16[8,32,384]{2,1,0:T(8,128)(2,1)} custom-call(bf16[8,32,384]{2,1,0:T(8,128)(2,1)} %bitcast.7, f32[1,384]{1,0:T(1,128)} %reshape.31.refs_1_, f32[1,384]{1,0:T(1,128)} %reshape.32.refs_2_, f32[16,128]{1,0:T(8,128)} %bitcast.8, f32[16,128]{1,0:T(8,128)} %bitcast.9, f32[1,384]{1,0:T(1,128)} %reshape.35.refs_5_, f32[16,128]{1,0:T(8,128)} %bitcast.10, ...), custom_call_target="tpu_custom_call" | custom-call | tf_op jit(solution)/shard_map/pallas_call | solution.py:254
  115.3 1.6 %copy.17 = bf16[256,384]{1,0:T(8,128)(2,1)} copy(bf16[256,384]{1,0:T(8,128)(2,1)} %bitcast.6) | data formatting | bytes 393216

commit v2 on v1

v2 whole, which is shorter than its diff:
```python
import functools
import jax
import jax.numpy as jnp
from jax import lax
from jax.experimental import pallas as pl
from jax.experimental.pallas import tpu as pltpu
from jax.sharding import PartitionSpec as P

MESH = pl.DeviceIdType.MESH
LANES = 128
CHUNK = 32
TIMES = (0.0, 1.5, 3.0, 4.5, 5.7, 6.9)


def kernel(cfg, *refs):
    ra, cb, chunk, chunks, width, hid, model, times = cfg
    (tok, gain1, gain2, gsc1, usc1, dsc1, gsc2, usc2, dsc2, g1, u1, d1, g2, u2, d2, out) = refs[:16]
    refs = refs[16:]
    far = ra // 2
    (fg, fu, fd, wgu, wd, stream, gains, gsc, usc, dsc, sqa, hb, load_sem) = refs[:13]
    refs = refs[13:]
    ysnd, yrcv, yown, zsnd, zrcv, zown, csnd, crcv = refs[:8]
    y_s, y_r, z_s, z_r, h_s, h_r, w_s, w_r, cb_s, cb_r = refs[8:]
    hl = hid // ra // LANES
    nl = 2 * hl

    me_r = lax.axis_index("ra")
    me_c = lax.axis_index("cb")
    bit, z = me_r % 2, me_r // 2
    pair = z * 2 + 1 - bit
    pos = bit * far + z
    z_of = [(z + d) % far for d in range(far)]
    c_of = [(me_c + d) % cb for d in range(cb)]
    loads = []
    for layer, (g, u, d) in enumerate(((g1, u1, d1), (g2, u2, d2))):
        for q, (src, dst) in enumerate(((g, fg), (u, fu), (d, fd))):
            copy = pltpu.make_async_copy(src, dst.at[layer], load_sem.at[layer * 3 + q])
            copy.start()
            loads.append(copy)

    barrier = pltpu.get_barrier_semaphore()
    pl.semaphore_signal(barrier, inc=1, device_id=(pair, me_c), device_id_type=MESH)
    for d in range(1, far):
        pl.semaphore_signal(barrier, inc=1, device_id=(z_of[d] * 2 + bit, me_c), device_id_type=MESH)
    for d in range(1, cb):
        pl.semaphore_signal(barrier, inc=1, device_id=(me_r, c_of[d]), device_id_type=MESH)

    stream[0] = tok[...]
    gains[0] = gain1[...]
    gains[1] = gain2[...]
    dsc[0] = dsc1[...] * 0.5
    dsc[1] = dsc2[...] * 0.5
    for src, dst, layer in ((gsc1, gsc, 0), (gsc2, gsc, 1), (usc1, usc, 0), (usc2, usc, 1)):
        for i in range(hid // LANES):
            dst[layer, i] = src[i : i + 1, :]

    def rev(j):
        return (j % far) * 2 + j // far

    hw = hl * LANES

    def convert_cols(layer, src, half):
        for j in range(ra):
            r = rev(j)
            wgu[layer, j, :, half * hw : (half + 1) * hw] = src[layer, :, r * hw : (r + 1) * hw].astype(jnp.bfloat16)

    def convert_down(layer):
        for j in range(ra):
            r = rev(j)
            wd[layer, j * hw : (j + 1) * hw, :] = fd[layer, r * hw : (r + 1) * hw, :].astype(jnp.bfloat16)

    loads[0].wait()
    convert_cols(0, fg, 0)
    loads[1].wait()
    convert_cols(0, fu, 1)
    pl.semaphore_wait(barrier, 1 + (far - 1) + (cb - 1))

    def remote(src, dst, send, recv, r, col):
        return pltpu.make_async_remote_copy(
            src_ref=src, dst_ref=dst, send_sem=send, recv_sem=recv, device_id=(r, col), device_id_type=MESH)

    def y_copy(c):
        return remote(ysnd.at[c], yrcv.at[c], y_s.at[c], y_r.at[c], pair, me_c)

    def z_copy(d, c):
        return remote(zsnd.at[d - 1, c], zrcv.at[d - 1, c], z_s.at[d - 1, c], z_r.at[d - 1, c], z_of[d] * 2 + bit, me_c)

    def h_copy(d, c):
        part = hb.at[c, pl.ds(pos * hl, hl)]
        return remote(part, part, h_s.at[d - 1, c], h_r.at[d - 1, c], z_of[d] * 2 + bit, me_c)

    def w_copy(c):
        part = hb.at[c, pl.ds(bit * (far * hl), far * hl)]
        return remote(part, part, w_s.at[c], w_r.at[c], pair, me_c)

    def cb_copy(d, i):
        return remote(csnd.at[i], crcv.at[i, me_c], cb_s.at[d - 1, i], cb_r.at[d - 1, i], me_r, c_of[d])

    def packed(sq):
        hi = sq.astype(jnp.bfloat16).astype(jnp.float32)
        lane = lax.broadcasted_iota(jnp.int32, sq.shape, 1)
        return jnp.where(lane < LANES // 2, hi, sq - hi).astype(jnp.bfloat16)

    def unpacked(v):
        v = v.astype(jnp.float32)
        return v + pltpu.roll(v, LANES // 2, 1)

    def first(layer, c):
        s = stream[layer, c].astype(jnp.float32)
        sq = jnp.broadcast_to(jnp.sum(s * s, axis=1, keepdims=True), (chunk, LANES))
        sqa[c] = sq
        ysnd[c, far * nl] = packed(sq)
        shaped = (s * gains[layer]).astype(jnp.bfloat16)
        half = ra // 2
        for jj in range(half):
            r = jnp.dot(shaped, wgu[layer, (1 - bit) * half + jj], preferred_element_type=jnp.float32)
            for q in range(nl):
                ysnd[c, jj * nl + q] = r[:, q * LANES : (q + 1) * LANES].astype(jnp.bfloat16)
        y_copy(c).start()
        for jj in range(half):
            r = jnp.dot(shaped, wgu[layer, bit * half + jj], preferred_element_type=jnp.float32)
            for q in range(nl):
                yown[c, jj * nl + q] = r[:, q * LANES : (q + 1) * LANES]

    def reduce(layer, c):
        y_copy(c).wait()
        sq = sqa[c] + unpacked(yrcv[c, far * nl])
        sqa[c] = sq
        square = packed(sq)
        for d in range(1, far):
            part = pl.ds(z_of[d] * nl, nl)
            zsnd[d - 1, c, 0:nl] = (yown[c, part] + yrcv[c, part].astype(jnp.float32)).astype(jnp.bfloat16)
            zsnd[d - 1, c, nl] = square
            z_copy(d, c).start()
        part = pl.ds(z * nl, nl)
        zown[c] = yown[c, part] + yrcv[c, part].astype(jnp.float32)

    def gate(layer, c):
        total = zown[c]
        sq = sqa[c]
        for d in range(1, far):
            z_copy(d, c).wait()
            total = total + zrcv[d - 1, c, 0:nl].astype(jnp.float32)
            sq = sq + unpacked(zrcv[d - 1, c, nl])
        inverse = lax.rsqrt(sq / model + 1e-06)[None]
        mine = pl.ds(me_r * hl, hl)
        g = inverse * gsc[layer, mine] * total[:hl]
        u = inverse * usc[layer, mine] * total[hl:]
        hidden = (g / (1.0 + jnp.exp(-g))) * u
        hb[c, pl.ds(pos * hl, hl)] = hidden.astype(jnp.bfloat16)
        for d in range(1, far):
            h_copy(d, c).start()

    def gather(layer, c):
        for d in range(1, far):
            h_copy(d, c).wait()
        w_copy(c).start()

    def down(layer, c):
        w_copy(c).wait()
        h = jnp.concatenate([hb[c, i] for i in range(hid // LANES)], axis=1)
        i = layer * chunks + c
        part = jnp.dot(h, wd[layer], preferred_element_type=jnp.float32).astype(jnp.bfloat16)
        csnd[i] = part
        crcv[i, me_c] = part
        for d in range(1, cb):
            cb_copy(d, i).start()

    def last(layer, c):
        i = layer * chunks + c
        for d in range(1, cb):
            cb_copy(d, i).wait()
        total = crcv[i, 0].astype(jnp.float32)
        for q in range(1, cb):
            total = total + crcv[i, q].astype(jnp.float32)
        s = stream[layer, c].astype(jnp.float32)
        stream[layer + 1, c] = (s + dsc[layer] * total).astype(jnp.bfloat16)

    stages = [first, reduce, gate, gather, down, last]
    lags = [int(x) for x in times]
    order = sorted(range(len(stages)), key=lambda s: times[s] - lags[s])
    shift = max(chunks, lags[-1] + 1)

    later = {
        0: lambda: (loads[2].wait(), convert_down(0)),
        1: lambda: (loads[3].wait(), convert_cols(1, fg, 0)),
        2: lambda: (loads[4].wait(), convert_cols(1, fu, 1)),
        3: lambda: (loads[5].wait(), convert_down(1)),
    }

    def tick(t, carry):
        for s in order:
            rel = t - lags[s]
            layer = jnp.where(rel >= shift, 1, 0)
            c = rel - layer * shift

            @pl.when((rel >= 0) & (c < chunks))
            def _(s=s, layer=layer, c=c):
                stages[s](layer, c)

        for at, act in later.items():
            @pl.when(t == at)
            def _(act=act):
                act()

        return carry

    lax.fori_loop(0, shift + chunks + lags[-1], tick, 0)
    out[...] = stream[2]


def fused(cfg, *args):
    ra, cb, chunk, chunks, width, hid, model, times = cfg
    far = ra // 2
    (tok, gain1, g1, u1, d1, gs1, us1, ds1, gain2, g2, u2, d2, gs2, us2, ds2) = args
    rows = hid // LANES
    nl = 2 * (hid // ra // LANES)
    bf, f32 = jnp.bfloat16, jnp.float32
    V = pltpu.VMEM
    D = pltpu.SemaphoreType.DMA
    scratch = [
        V((2, width, hid), f32),
        V((2, width, hid), f32),
        V((2, hid, width), f32),
        V((2, ra, width, nl * LANES), bf),
        V((2, hid, width), bf),
        V((3, chunks, chunk, width), bf),
        V((2, 1, width), f32),
        V((2, rows, 1, LANES), f32),
        V((2, rows, 1, LANES), f32),
        V((2, 1, width), f32),
        V((chunks, chunk, LANES), f32),
        V((chunks, rows, chunk, LANES), bf),
        D((6,)),
    ]
    scratch += [V((chunks, far * nl + 1, chunk, LANES), bf), V((chunks, far * nl + 1, chunk, LANES), bf)]
    scratch += [V((chunks, far * nl, chunk, LANES), f32)]
    scratch += [V((far - 1, chunks, nl + 1, chunk, LANES), bf), V((far - 1, chunks, nl + 1, chunk, LANES), bf)]
    scratch += [V((chunks, nl, chunk, LANES), f32)]
    scratch += [V((2 * chunks, chunk, width), bf), V((2 * chunks, cb, chunk, width), bf)]
    scratch += [D((chunks,))] * 2 + [D((far - 1, chunks))] * 4 + [D((chunks,))] * 2 + [D((cb - 1, 2 * chunks))] * 2
    vm = pl.BlockSpec(memory_space=pltpu.VMEM)
    hbm = pl.BlockSpec(memory_space=pl.ANY)
    result = pl.pallas_call(
        functools.partial(kernel, cfg),
        out_shape=jax.ShapeDtypeStruct((chunks, chunk, width), bf),
        in_specs=[vm] * 9 + [hbm] * 6,
        out_specs=vm,
        scratch_shapes=scratch,
        compiler_params=pltpu.CompilerParams(collective_id=0, has_side_effects=True, vmem_limit_bytes=64 * 1000 * 1000),
    )(
        tok.reshape(chunks, chunk, width),
        gain1.reshape(1, width), gain2.reshape(1, width),
        gs1.reshape(rows, LANES), us1.reshape(rows, LANES), ds1.reshape(1, width),
        gs2.reshape(rows, LANES), us2.reshape(rows, LANES), ds2.reshape(1, width),
        g1, u1, d1, g2, u2, d2,
    )
    return result.reshape(chunks * chunk, width)


def plain_half(model, s_in, gain, w_gate, w_up, w_down, gate_scale, up_scale, down_scale):
    stream = s_in.astype(jnp.float32)
    squares = jnp.sum(stream * stream, axis=1)
    shaped = (stream * gain[None, :]).astype(jnp.bfloat16)
    gate_part = jnp.dot(shaped, w_gate.astype(jnp.bfloat16), preferred_element_type=jnp.float32)
    up_part = jnp.dot(shaped, w_up.astype(jnp.bfloat16), preferred_element_type=jnp.float32)
    squares, gate_sum, up_sum = lax.psum((squares, gate_part, up_part), "ra")
    inverse = lax.rsqrt(squares / model + 1e-06)[:, None]
    gate_full = inverse * gate_scale[None, :] * gate_sum
    up_full = inverse * up_scale[None, :] * up_sum
    hidden = (jax.nn.silu(gate_full) * up_full).astype(jnp.bfloat16)
    down_part = jnp.dot(hidden, w_down.astype(jnp.bfloat16), preferred_element_type=jnp.float32)
    down_sum = lax.psum(down_part, "cb")
    return (stream + 0.5 * down_scale[None, :] * down_sum).astype(jnp.bfloat16)


def solution(mesh):
    ra, cb = mesh.shape["ra"], mesh.shape["cb"]

    def body(*args):
        tokens, width = args[0].shape
        hid = args[2].shape[1]
        even = ra % 2 == 0 and ra > 2 and cb > 1
        if even and hid % (ra * LANES) == 0 and width % LANES == 0 and tokens % CHUNK == 0:
            cfg = (ra, cb, CHUNK, tokens // CHUNK, width, hid, width * ra, TIMES)
            return fused(cfg, *args)
        middle = plain_half(width * ra, *args[:8])
        return plain_half(width * ra, middle, *args[8:])

    col, grid, turned = P("ra"), P("ra", "cb"), P("cb", "ra")
    sub = (col, grid, grid, turned, P("cb"), P("cb"), col)
    return jax.shard_map(
        body, mesh=mesh, in_specs=(P(None, "ra"),) + sub + sub, out_specs=P(None, "ra"), check_vma=False)
```

time: 117 us -> 110 us (0.940)
  Pallas kernels: 110 us -> 103 us
    pallas_call x1, Pallas kernels: 110 us -> 103 us  [fused(): pl.pallas_call(functools.partial(kernel, cfg), out_shape=jax.ShapeDtypeSt...]
where the time goes in v2:
time: 110 us
  Pallas kernels  103 us (94%)
  local copies, waits for them, and re-layouts  6.61 us (6%)
    pallas_call x1, Pallas kernels, fused(): pl.pallas_call(functools.partial(kernel, cfg), out_shape=jax.ShapeDtypeSt...  103 us

profile of v2, /device:TPU:0, one launch (start us, length us, event | category | flops | bytes accessed | tf_op | source)
XLA Modules:
  0.0 110.0 jit_solution(13727750922423525114)
XLA Ops:
  0.0 1.2 %reshape.31.refs_1_ = f32[1,384]{1,0:T(1,128)} reshape(f32[384]{0:T(512)} %param.16) | data formatting | bytes 3072 | tf_op jit(solution)/shard_map/reshape | solution.py:253
  1.2 1.2 %reshape.35.refs_5_ = f32[1,384]{1,0:T(1,128)} reshape(f32[384]{0:T(512)} %param.22) | data formatting | bytes 3072 | tf_op jit(solution)/shard_map/reshape | solution.py:254
  2.5 1.3 %reshape.32.refs_2_ = f32[1,384]{1,0:T(1,128)} reshape(f32[384]{0:T(512)} %param.23) | data formatting | bytes 3072 | tf_op jit(solution)/shard_map/reshape | solution.py:253
  3.7 1.2 %reshape.38.refs_8_ = f32[1,384]{1,0:T(1,128)} reshape(f32[384]{0:T(512)} %param.29) | data formatting | bytes 3072 | tf_op jit(solution)/shard_map/reshape | solution.py:255
  5.0 103.4 %shard_map.145 = bf16[8,32,384]{2,1,0:T(8,128)(2,1)} custom-call(bf16[8,32,384]{2,1,0:T(8,128)(2,1)} %bitcast.7, f32[1,384]{1,0:T(1,128)} %reshape.31.refs_1_, f32[1,384]{1,0:T(1,128)} %reshape.32.refs_2_, f32[16,128]{1,0:T(8,128)} %bitcast.8, f32[16,128]{1,0:T(8,128)} %bitcast.9, f32[1,384]{1,0:T(1,128)} %reshape.35.refs_5_, f32[16,128]{1,0:T(8,128)} %bitcast.10, ...), custom_call_target="tpu_custom_call" | custom-call | tf_op jit(solution)/shard_map/pallas_call | solution.py:244
  108.4 1.6 %copy.17 = bf16[256,384]{1,0:T(8,128)(2,1)} copy(bf16[256,384]{1,0:T(8,128)(2,1)} %bitcast.6) | data formatting | bytes 393216
